TPU v7x, 32 devices: a whole 2x2x4 slice. The times are simulated.
32 devices in a mesh: sp: 4 (over y, x), tp: 8 (over z, core).
Axes of the slice: x: 2, y: 2, z: 4, core: 2. Of those that a mesh axis runs over, the one named last changes fastest.
Arguments:
- moe_input: bfloat16 [1024, 4096], P('sp', 'tp'), may hold values from -6 to 6
- out_gate: bfloat16 [1024, 4096], P('sp', 'tp'), may hold values from -6 to 6
- in_gate: bfloat16 [1024, 4096], P('sp', 'tp'), may hold values from -6 to 6
- values: bfloat16 [1024, 4096], P('sp', 'tp'), may hold values from -6 to 6
- conv_taps: float32 [3, 4096], P(None, 'tp'), may hold values from -3 to 3
- out_proj: bfloat16 [4096, 4096], P(None, 'tp'), may hold values from -0.09375 to 0.09375
- route_ids: int32 [1024, 2], P('sp'), may hold values from 0 to 3, all different within a row; in each aligned block of 256 rows (0 to 255, 256 to 511, ...) at most 192 rows name the same one
- route_gates: float32 [1024, 2], P('sp'), may hold values from 0.1 to 0.9
- expert_gate: bfloat16 [4, 4096, 2048], P('sp', None, 'tp'), may hold values from -0.09375 to 0.09375
- expert_up: bfloat16 [4, 4096, 2048], P('sp', None, 'tp'), may hold values from -0.09375 to 0.09375
- expert_down: bfloat16 [4, 2048, 4096], P('sp', 'tp'), may hold values from -0.125 to 0.125
- cotangent: bfloat16 [1024, 4096], P('sp', 'tp'), may hold values from -6 to 6
Outputs:
- grad_out_gate: bfloat16 [1024, 4096], P('sp', 'tp')
- grad_in_gate: bfloat16 [1024, 4096], P('sp', 'tp')
- grad_values: bfloat16 [1024, 4096], P('sp', 'tp')
- grad_out_proj: float32 [4096, 4096], P('sp', 'tp')
- grad_expert_gate: float32 [4, 4096, 2048], P('sp', None, 'tp')
- grad_expert_up: float32 [4, 4096, 2048], P('sp', None, 'tp')
- grad_expert_down: float32 [4, 2048, 4096], P('sp', 'tp')
Inputs may be any that keep to these rules, and one draw needn't show every extreme that they name: `route_ids`: the 2 experts of a token differ. In the rows of one device no expert is named by more than 192 assignments, and in some device's rows some expert is named by exactly 192.
All inputs are finite; a program needn't handle non-finite values.
Results may differ from a plain program's by a relative error of at most 0.014.
Values may be sent and summed in bfloat16 or wider, within the bound.
A program may use at most 128 MiB of HBM per device.

v0:
```python
import jax
import jax.numpy as jnp
from jax import lax
from jax.sharding import PartitionSpec as P


def padded(array, sides, width):
    for axis, dim in sides:
        size, length = (lax.axis_size(axis), array.shape[dim])
        up = [(i, (i + 1) % size) for i in range(size - 1)]
        down = [(j, i) for i, j in up]
        last = lax.slice_in_dim(array, length - width, length, axis=dim)
        initial = lax.slice_in_dim(array, 0, width, axis=dim)
        before = lax.ppermute(last, axis, up)
        after = lax.ppermute(initial, axis, down)
        array = jnp.concatenate([before, array, after], axis=dim)
    return array


def body(
    moe_input,
    out_gate,
    in_gate,
    values,
    conv_taps,
    out_proj,
    route_ids,
    route_gates,
    expert_gate,
    expert_up,
    expert_down,
    cotangent,
):
    token_count = moe_input.shape[0]
    part_width = moe_input.shape[1]
    pick_count = route_ids.shape[1]
    group_count = lax.axis_size("sp")
    local_count = expert_gate.shape[0]
    expert_count = group_count * local_count
    capacity = 3 * token_count // expert_count
    contract_rows = (((0,), (0,)), ((), ()))
    flat_ids = route_ids.reshape(-1)
    owner = jnp.arange(token_count * pick_count, dtype=jnp.int32) // pick_count
    one_hot = (flat_ids[:, None] == jnp.arange(expert_count, dtype=jnp.int32)[None, :]).astype(
        jnp.int32
    )
    earlier = jnp.cumsum(one_hot, axis=0) - one_hot
    position = jnp.sum(earlier * one_hot, axis=1)
    slot_index = flat_ids * capacity + position
    slot_token = (
        jnp.full((expert_count * capacity,), token_count, jnp.int32).at[slot_index].set(owner)
    )
    slot_weight = (
        jnp.zeros((expert_count * capacity,), jnp.float32)
        .at[slot_index]
        .set(route_gates.reshape(-1))
    )
    padded_input = jnp.concatenate([moe_input, jnp.zeros((1, part_width), moe_input.dtype)], axis=0)
    padded_cot = jnp.concatenate([cotangent, jnp.zeros((1, part_width), cotangent.dtype)], axis=0)
    send_rows = padded_input[slot_token].reshape(expert_count, capacity, part_width)
    send_cot = (slot_weight[:, None] * padded_cot[slot_token].astype(jnp.float32)).astype(
        jnp.bfloat16
    )
    send_cot = send_cot.reshape(expert_count, capacity, part_width)
    recv_rows, recv_cot = (
        lax.all_to_all(send_rows, "sp", split_axis=0, concat_axis=1, tiled=True),
        lax.all_to_all(send_cot, "sp", split_axis=0, concat_axis=1, tiled=True),
    )
    full_rows, full_cot = (
        lax.all_gather(recv_rows, "tp", axis=2, tiled=True),
        lax.all_gather(recv_cot, "tp", axis=2, tiled=True),
    )
    pre_gate = jnp.einsum(
        "prd,pdf->prf", full_rows, expert_gate, preferred_element_type=jnp.float32
    )
    pre_up = jnp.einsum("prd,pdf->prf", full_rows, expert_up, preferred_element_type=jnp.float32)
    gate_sig = jax.nn.sigmoid(pre_gate)
    activated = pre_gate * gate_sig
    hidden_act = (activated * pre_up).astype(jnp.bfloat16)
    grad_expert_down = jnp.einsum(
        "prf,prd->pfd", hidden_act, full_cot, preferred_element_type=jnp.float32
    )
    grad_hidden = jnp.einsum(
        "prd,pfd->prf", full_cot, expert_down, preferred_element_type=jnp.float32
    )
    grad_pre_gate = (grad_hidden * pre_up * gate_sig * (1.0 + pre_gate * (1.0 - gate_sig))).astype(
        jnp.bfloat16
    )
    grad_pre_up = (grad_hidden * activated).astype(jnp.bfloat16)
    grad_expert_gate = jnp.einsum(
        "prd,prf->pdf", full_rows, grad_pre_gate, preferred_element_type=jnp.float32
    )
    grad_expert_up = jnp.einsum(
        "prd,prf->pdf", full_rows, grad_pre_up, preferred_element_type=jnp.float32
    )
    partial_grad = jnp.einsum(
        "prf,pdf->prd", grad_pre_gate, expert_gate, preferred_element_type=jnp.float32
    ) + jnp.einsum("prf,pdf->prd", grad_pre_up, expert_up, preferred_element_type=jnp.float32)
    slot_grad = lax.psum_scatter(partial_grad, "tp", scatter_dimension=2, tiled=True)
    returned = lax.all_to_all(slot_grad, "sp", split_axis=1, concat_axis=0, tiled=True)
    flat_returned = returned.reshape(expert_count * capacity, part_width)
    moe_grad = jnp.sum(
        flat_returned[slot_index].reshape(token_count, pick_count, part_width), axis=1
    )
    mixer_cot = (cotangent.astype(jnp.float32) + moe_grad).astype(jnp.bfloat16)
    conv_in = in_gate.astype(jnp.float32) * values.astype(jnp.float32)
    rimmed = padded(conv_in, (("sp", 0),), 1)
    conv_out = rimmed[:-2] * conv_taps[0] + rimmed[1:-1] * conv_taps[1] + rimmed[2:] * conv_taps[2]
    mixed = (out_gate.astype(jnp.float32) * conv_out).astype(jnp.bfloat16)
    full_mixer_cot = lax.all_gather(mixer_cot, "tp", axis=1, tiled=True)
    grad_mixed = jnp.dot(full_mixer_cot, out_proj, preferred_element_type=jnp.float32)
    grad_out_gate = (grad_mixed * conv_out).astype(jnp.bfloat16)
    grad_conv_out = grad_mixed * out_gate.astype(jnp.float32)
    rim_grad = padded(grad_conv_out, (("sp", 0),), 1)
    grad_conv_in = (
        rim_grad[2:] * conv_taps[0] + rim_grad[1:-1] * conv_taps[1] + rim_grad[:-2] * conv_taps[2]
    )
    grad_in_gate = (grad_conv_in * values.astype(jnp.float32)).astype(jnp.bfloat16)
    grad_values = (grad_conv_in * in_gate.astype(jnp.float32)).astype(jnp.bfloat16)
    columns = lax.all_to_all(full_mixer_cot, "sp", split_axis=1, concat_axis=0, tiled=True)
    grad_out_proj = lax.dot_general(
        columns,
        lax.all_gather(mixed, "sp", axis=0, tiled=True),
        contract_rows,
        preferred_element_type=jnp.float32,
    )
    return (
        grad_out_gate,
        grad_in_gate,
        grad_values,
        grad_out_proj,
        grad_expert_gate,
        grad_expert_up,
        grad_expert_down,
    )


def solution(mesh):
    return jax.shard_map(
        body,
        mesh=mesh,
        in_specs=(
            P("sp", "tp"),
            P("sp", "tp"),
            P("sp", "tp"),
            P("sp", "tp"),
            P(None, "tp"),
            P(None, "tp"),
            P("sp", None),
            P("sp", None),
            P("sp", None, "tp"),
            P("sp", None, "tp"),
            P("sp", "tp", None),
            P("sp", "tp"),
        ),
        out_specs=(
            P("sp", "tp"),
            P("sp", "tp"),
            P("sp", "tp"),
            P("sp", "tp"),
            P("sp", None, "tp"),
            P("sp", None, "tp"),
            P("sp", "tp", None),
        ),
        check_vma=False,
    )
```

profile of v0, /device:TPU:0, one launch (start us, length us, event | category | flops | bytes accessed | tf_op | source)
XLA Modules:
  0.0 423.8 jit_solution(5555244624679812317)
XLA Ops:
  14.7 2.7 gather_fusion.1
  17.4 16.6 %all_to_all.52 = bf16[4,192,512]{2,1,0:T(8,128)(2,1)} all-to-all(bf16[4,192,512]{2,1,0:T(8,128)(2,1)S(1)} %bitcast.94), channel_id=1, replica_groups=mesh['sp'=4,'tp'=8] {'sp'}, dimensions={0} | all-to-all | bytes 1572864 | tf_op jit(solution)/shard_map/all_to_all | solution.py:66
  36.9 2.7 gather_fusion
  39.8 13.3 %all_to_all.53 = bf16[4,192,512]{2,1,0:T(8,128)(2,1)} all-to-all(bf16[4,192,512]{2,1,0:T(8,128)(2,1)S(1)} %fusion.27), channel_id=1, replica_groups=mesh['sp'=4,'tp'=8] {'sp'}, dimensions={0} | all-to-all | bytes 1572864 | tf_op jit(solution)/shard_map/all_to_all | solution.py:67
  53.3 45.2 %all-gather.7.cloned.1.call-done = bf16[1,768,4096]{2,1,0:T(8,128)(2,1)} async-done(((bf16[1,768,512]{2,1,0:T(8,128)(2,1)}), bf16[1,768,4096]{2,1,0:T(8,128)(2,1)}) %all-gather.7.cloned.1.call-update) | async-done | bytes 6291472 | tf_op jit(solution)/shard_map/all_gather | solution.py:70
  98.5 4.7 %fusion.4 = f32[768,256]{1,0:T(8,128)S(1)} fusion(bf16[1,768,4096]{2,1,0:T(8,128)(2,1)} %all-gather.7.cloned.1.call-done, bf16[1,4096,256]{2,1,0:T(8,128)(2,1)S(1)} %copy-done), kind=kOutput, calls=%fused_computation.10 | convolution fusion | flops 1610612736 | bytes 9175040 | tf_op jit(solution)/shard_map/prd,pdf->prf/dot_general | solution.py:73
  103.8 2.7 fusion.6
  106.4 57.1 %all-gather.5.cloned.1.call-done = bf16[1,768,4096]{2,1,0:T(8,128)(2,1)} async-done(((bf16[1,768,512]{2,1,0:T(8,128)(2,1)}), bf16[1,768,4096]{2,1,0:T(8,128)(2,1)}) %all-gather.5.cloned.1.call-update) | async-done | bytes 6291472 | tf_op jit(solution)/shard_map/all_gather | solution.py:71
  163.5 5.5 %multiply_convert_fusion.1 = (bf16[768,256]{1,0:T(8,128)(2,1)S(1)}, bf16[768,256]{1,0:T(8,128)(2,1)S(1)}) fusion(f32[768,256]{1,0:T(8,128)S(1)} %fusion.4, f32[768,256]{1,0:T(8,128)} %fusion.6, bf16[1,256,4096]{2,1,0:T(8,128)(2,1)} %param.22, bf16[1,768,4096]{2,1,0:T(8,128)(2,1)} %all-gather.5.cloned.1.call-done), kind=kOutput, calls=%fused_computation.31 | convolution fusion | flops 1613168640 | bytes 10747904 | tf_op jit(solution)/shard_map/prd,pfd->prf/dot_general | solution.py:83
  170.9 6.5 %add_bitcast_fusion = f32[1,768,4096]{2,1,0:T(8,128)} fusion(f32[768,4096]{1,0:T(8,128)S(1)} %fusion.21, bf16[768,256]{1,0:T(8,128)(2,1)S(1)} %get-tuple-element.7, bf16[1,4096,256]{2,1,0:T(8,128)(2,1)S(1)} %copy-done.3), kind=kOutput, calls=%fused_computation.5 | convolution fusion | flops 1613758464 | bytes 27656192 | tf_op jit(solution)/shard_map/prf,pdf->prd/dot_general | solution.py:98
  177.5 127.9 %reduce-scatter.2.cloned.1.call-done = f32[1,768,512]{2,1,0:T(8,128)} async-done(((f32[1,768,4096]{2,1,0:T(8,128)}), f32[1,768,512]{2,1,0:T(8,128)}) %reduce-scatter.2.cloned.1.call-update) | async-done | bytes 1572880 | tf_op jit(solution)/shard_map/reduce_scatter | solution.py:99
  305.4 4.2 copy.33
  309.6 4.3 %all-to-all-start.2 = ((f32[1,768,512]{2,0,1:T(1,128)}), f32[1,768,512]{2,0,1:T(1,128)}, u32[]{:S(2)}, u32[]{:S(2)}) async-start(f32[1,768,512]{2,0,1:T(1,128)} %copy.33), calls=%async_computation.3 | async-start | bytes 3145728 | tf_op jit(solution)/shard_map/all_to_all | solution.py:100
  314.2 17.4 %all-to-all-done.2 = f32[1,768,512]{2,0,1:T(1,128)} async-done(((f32[1,768,512]{2,0,1:T(1,128)}), f32[1,768,512]{2,0,1:T(1,128)}, u32[]{:S(2)}, u32[]{:S(2)}) %all-to-all-start.2) | async-done | bytes 1572896 | tf_op jit(solution)/shard_map/all_to_all | solution.py:100
  337.7 3.3 collective-permute-start
  343.2 7.0 %fusion.12 = f32[1,256,4096]{2,1,0:T(8,128)} fusion(bf16[1,768,4096]{2,1,0:T(8,128)(2,1)} %all-gather.5.cloned.1.call-done, f32[768,256]{1,0:T(8,128)S(1)} %copy-done.7, f32[768,256]{1,0:T(8,128)S(1)} %copy-done.6), kind=kOutput, calls=%fused_computation.18 | convolution fusion | flops 1611792384 | bytes 12058624 | tf_op jit(solution)/shard_map/prf,prd->pfd/dot_general | solution.py:80
  350.2 16.1 %all-gather.9.cloned.1.call-done = bf16[256,4096]{1,0:T(8,128)(2,1)} async-done(((bf16[256,512]{1,0:T(8,128)(2,1)}), bf16[256,4096]{1,0:T(8,128)(2,1)}) %all-gather.9.cloned.1.call-update) | async-done | bytes 2097168 | tf_op jit(solution)/shard_map/all_gather | solution.py:110
  366.3 5.6 %fusion.31 = (bf16[256,512]{1,0:T(8,128)(2,1)}, bf16[256,512]{1,0:T(8,128)(2,1)}, f32[256,512]{1,0:T(8,128)S(1)}) fusion(bf16[256,512]{1,0:T(8,128)(2,1)} %param.13, f32[512]{0:T(512)S(1)} %bitcast.100, f32[1,512]{1,0:T(1,128)} %copy-done.18, f32[256,512]{1,0:T(8,128)} %copy-done.13, f32[512]{0:T(512)S(1)} %bitcast.102, f32[512]{0:T(512)S(1)} %bitcast.98, ...), kind=kOutput, calls=%fused_computation.42 | convolution fusion | flops 1075445760 | bytes 8136704 | tf_op jit(solution)/shard_map/dot_general | solution.py:111
  374.4 3.6 all-to-all-start.3
  378.0 6.8 %fusion.18 = f32[1,4096,256]{2,1,0:T(8,128)} fusion(bf16[768,256]{1,0:T(8,128)(2,1)S(1)} %get-tuple-element.7, bf16[1,768,4096]{2,1,0:T(8,128)(2,1)} %all-gather.7.cloned.1.call-done), kind=kOutput, calls=%fused_computation.20 | convolution fusion | flops 1610612736 | bytes 10878976 | tf_op jit(solution)/shard_map/prd,prf->pdf/dot_general | solution.py:93
  386.2 4.7 %collective-permute-start.3 = (f32[1,512]{1,0:T(1,128)S(1)}, f32[1,512]{1,0:T(1,128)S(1)}, u32[]{:S(2)}, u32[]{:S(2)}) collective-permute-start(f32[1,512]{1,0:T(1,128)S(1)} %get-tuple-element.15), channel_id=1, source_target_pairs={{0,8},{8,16},{16,24},{1,9},{9,17},{17,25},{2,10},{10,18},{18,26},{... | collective-permute-start | bytes 6152 | tf_op jit(solution)/shard_map/ppermute | solution.py:14
  390.9 6.7 %fusion.15 = f32[1,4096,256]{2,1,0:T(8,128)} fusion(bf16[768,256]{1,0:T(8,128)(2,1)S(1)} %copy-done.15, bf16[1,768,4096]{2,1,0:T(8,128)(2,1)} %all-gather.7.cloned.1.call-done), kind=kOutput, calls=%fused_computation.19 | convolution fusion | flops 1610612736 | bytes 10878976 | tf_op jit(solution)/shard_map/prd,prf->pdf/dot_general | solution.py:90
  397.5 11.6 %collective-permute-done.2 = f32[1,512]{1,0:T(1,128)S(1)} collective-permute-done((f32[1,512]{1,0:T(1,128)S(1)}, f32[1,512]{1,0:T(1,128)S(1)}, u32[]{:S(2)}, u32[]{:S(2)}) %collective-permute-start.2) | collective-permute-done | bytes 2080 | tf_op jit(solution)/shard_map/ppermute | solution.py:15
  412.7 4.6 %fusion.56 = f32[1024,512]{1,0:T(8,128)} fusion(bf16[1024,1024]{1,0:T(8,128)(2,1)} %bitcast.97, bf16[1024,512]{1,0:T(8,128)(2,1)} %all-gather.11.cloned.1.call-done), kind=kOutput, calls=%fused_computation.86 | convolution fusion | flops 1073741824 | bytes 5242880 | tf_op jit(solution)/shard_map/dot_general | solution.py:121
  (93 shorter events, 28.8 us)
Async XLA Ops:
  7.2 91.4 %copy-start = (bf16[1,4096,256]{2,1,0:T(8,128)(2,1)S(1)}, bf16[1,4096,256]{2,1,0:T(8,128)(2,1)}, u32[]{:S(2)}) copy-start(bf16[1,4096,256]{2,1,0:T(8,128)(2,1)} %param.20) | copy-start | bytes 6291460
  7.2 91.3 %all-gather.7.cloned.1.call-start = ((), (), s32[]{:S(2)}) async-start(), calls=%async_computation.6 | async-start | bytes 7077888 | tf_op jit(solution)/shard_map/all_gather | solution.py:70
  17.4 16.7 %copy-start.16 = (f32[256,2]{0,1:T(2,128)S(1)}, f32[256,2]{0,1:T(2,128)}, u32[]{:S(2)}) copy-start(f32[256,2]{0,1:T(2,128)} %param.19) | copy-start | bytes 6148
  17.4 19.5 %copy-start.8 = (bf16[256,512]{1,0:T(8,128)(2,1)S(1)}, bf16[256,512]{1,0:T(8,128)(2,1)}, u32[]{:S(2)}) copy-start(bf16[256,512]{1,0:T(8,128)(2,1)} %param.23) | copy-start | bytes 786436
  34.0 129.5 %all-gather.5.cloned.1.call-start = ((), (), s32[]{:S(2)}) async-start(), calls=%async_computation.5 | async-start | bytes 7077888 | tf_op jit(solution)/shard_map/all_gather | solution.py:71
  53.1 252.3 %reduce-scatter.2.cloned.1.call-start = ((), (), s32[]{:S(2)}) async-start(), calls=%async_computation.7 | async-start | bytes 14155776 | tf_op jit(solution)/shard_map/reduce_scatter | solution.py:99
  98.5 4.7 %copy-start.2 = (bf16[1,4096,256]{2,1,0:T(8,128)(2,1)S(1)}, bf16[1,4096,256]{2,1,0:T(8,128)(2,1)}, u32[]{:S(2)}) copy-start(bf16[1,4096,256]{2,1,0:T(8,128)(2,1)} %param.21) | copy-start | bytes 6291460
  98.5 5.2 %copy-start.17 = (bf16[1,768,4096]{2,1,0:T(8,128)(2,1)S(1)}, bf16[1,768,4096]{2,1,0:T(8,128)(2,1)}, u32[]{:S(2)}) copy-start(bf16[1,768,4096]{2,1,0:T(8,128)(2,1)} %all-gather.7.cloned.1.call-done) | copy-start | bytes 18874372
  103.8 59.7 %copy-start.5 = (f32[768,256]{1,0:T(8,128)}, f32[768,256]{1,0:T(8,128)S(1)}, u32[]{:S(2)}) copy-start(f32[768,256]{1,0:T(8,128)S(1)} %fusion.4) | copy-start | bytes 2359300
  309.6 22.1 %all-to-all-start.2 = ((f32[1,768,512]{2,0,1:T(1,128)}), f32[1,768,512]{2,0,1:T(1,128)}, u32[]{:S(2)}, u32[]{:S(2)}) async-start(f32[1,768,512]{2,0,1:T(1,128)} %copy.33), calls=%async_computation.3 | async-start | bytes 3145728 | tf_op jit(solution)/shard_map/all_to_all | solution.py:100
  313.9 52.3 %all-gather.9.cloned.1.call-start = ((), (), s32[]{:S(2)}) async-start(), calls=%async_computation.8 | async-start | bytes 2359296 | tf_op jit(solution)/shard_map/all_gather | solution.py:110
  335.5 7.7 %copy-start.6 = (f32[768,256]{1,0:T(8,128)S(1)}, f32[768,256]{1,0:T(8,128)}, u32[]{:S(2)}) copy-start(f32[768,256]{1,0:T(8,128)} %copy-done.5) | copy-start | bytes 2359300
  336.8 6.4 %copy-start.7 = (f32[768,256]{1,0:T(8,128)S(1)}, f32[768,256]{1,0:T(8,128)}, u32[]{:S(2)}) copy-start(f32[768,256]{1,0:T(8,128)} %fusion.6) | copy-start | bytes 2359300
  337.6 75.1 %all-gather.11.cloned.1.call-start = ((), (), s32[]{:S(2)}) async-start(), calls=%async_computation.9 | async-start | bytes 1310720 | tf_op jit(solution)/shard_map/all_gather | solution.py:123
  337.7 12.5 %copy-start.13 = (f32[256,512]{1,0:T(8,128)}, f32[256,512]{1,0:T(8,128)S(1)}, u32[]{:S(2)}) copy-start(f32[256,512]{1,0:T(8,128)S(1)} %convert_multiply_fusion.4) | copy-start | bytes 1572868
  337.7 12.5 %collective-permute-start = (f32[1,512]{1,0:T(1,128)S(1)}, f32[1,512]{1,0:T(1,128)S(1)}, u32[]{:S(2)}, u32[]{:S(2)}) collective-permute-start(f32[1,512]{1,0:T(1,128)S(1)} %get-tuple-element.16), channel_id=1, source_target_pairs={{0,8},{8,16},{16,24},{1,9},{9,17},{17,25},{2,10},{10,18},{18,26},{... | collective-permute-start | bytes 6152 | tf_op jit(solution)/shard_map/ppermute | solution.py:14
  341.1 9.1 %collective-permute-start.1 = (f32[1,512]{1,0:T(1,128)S(1)}, f32[1,512]{1,0:T(1,128)S(1)}, u32[]{:S(2)}, u32[]{:S(2)}) collective-permute-start(f32[1,512]{1,0:T(1,128)S(1)} %get-tuple-element.17), channel_id=1, source_target_pairs={{8,0},{16,8},{24,16},{9,1},{17,9},{25,17},{10,2},{18,10},{26,18},{... | collective-permute-start | bytes 6152 | tf_op jit(solution)/shard_map/ppermute | solution.py:15
  350.2 16.1 %copy-start.18 = (f32[1,512]{1,0:T(1,128)}, f32[1,512]{1,0:T(1,128)S(1)}, u32[]{:S(2)}) copy-start(f32[1,512]{1,0:T(1,128)S(1)} %collective-permute-done.1) | copy-start | bytes 6148
  366.3 5.6 %copy-start.4 = (bf16[256,4096]{1,0:T(8,128)(2,1)S(1)}, bf16[256,4096]{1,0:T(8,128)(2,1)}, u32[]{:S(2)}) copy-start(bf16[256,4096]{1,0:T(8,128)(2,1)} %all-gather.9.cloned.1.call-done) | copy-start | bytes 6291460
  374.4 35.8 %all-to-all-start.3 = ((bf16[256,4,1024]{0,2,1:T(8,128)(2,1)}), bf16[256,4,1024]{0,2,1:T(8,128)(2,1)S(1)}, u32[]{:S(2)}, u32[]{:S(2)}) async-start(bf16[256,4,1024]{0,2,1:T(8,128)(2,1)} %bitcast.92), calls=%async_computation.4 | async-start | bytes 4194304 | tf_op jit(solution)/shard_map/all_to_all | solution.py:120
  378.0 12.8 %copy-start.15 = (bf16[768,256]{1,0:T(8,128)(2,1)S(1)}, bf16[768,256]{1,0:T(8,128)(2,1)}, u32[]{:S(2)}) copy-start(bf16[768,256]{1,0:T(8,128)(2,1)} %copy-done.14) | copy-start | bytes 1179652
  384.9 24.3 %collective-permute-start.2 = (f32[1,512]{1,0:T(1,128)S(1)}, f32[1,512]{1,0:T(1,128)S(1)}, u32[]{:S(2)}, u32[]{:S(2)}) collective-permute-start(f32[1,512]{1,0:T(1,128)S(1)} %get-tuple-element.14), channel_id=1, source_target_pairs={{8,0},{16,8},{24,16},{9,1},{17,9},{25,17},{10,2},{18,10},{26,18},{... | collective-permute-start | bytes 6152 | tf_op jit(solution)/shard_map/ppermute | solution.py:15
  386.2 23.0 %copy-start.11 = (bf16[256,512]{1,0:T(8,128)(2,1)S(1)}, bf16[256,512]{1,0:T(8,128)(2,1)}, u32[]{:S(2)}) copy-start(bf16[256,512]{1,0:T(8,128)(2,1)} %param.15) | copy-start | bytes 786436
  386.2 23.0 %collective-permute-start.3 = (f32[1,512]{1,0:T(1,128)S(1)}, f32[1,512]{1,0:T(1,128)S(1)}, u32[]{:S(2)}, u32[]{:S(2)}) collective-permute-start(f32[1,512]{1,0:T(1,128)S(1)} %get-tuple-element.15), channel_id=1, source_target_pairs={{0,8},{8,16},{16,24},{1,9},{9,17},{17,25},{2,10},{10,18},{18,26},{... | collective-permute-start | bytes 6152 | tf_op jit(solution)/shard_map/ppermute | solution.py:14
  (6 other events, 15.2 us)
Sparse Core Ops, SparseCore 0:
  34.1 64.3 all-gather.6
  100.1 63.3 all-gather.4
  177.6 127.7 reduce-scatter.1
  337.7 28.5 all-gather.8
  372.0 40.1 all-gather.10
where the time goes:
time: 425 us; the launch traced here: 424 us
  waiting for transfers between devices  275 us (65%)
  matrix products  52 us (12%)
  blocking collectives  29.8 us (7%)
  local copies, waits for them, and re-layouts  27.5 us (6%)
  starting transfers between devices  19.2 us (5%)
  between operations  14.2 us (3%)
  other arithmetic  5.71 us (1%)
    reduce_scatter x1, waiting for transfers between devices, body(): lax.psum_scatter(partial_grad, 'tp', scatter_dimension=2, tiled=True)  128 us
    all_gather x1, waiting for transfers between devices, body(): lax.all_gather(recv_cot, 'tp', axis=2, tiled=True)  57.1 us
    all_gather x1, waiting for transfers between devices, body(): lax.all_gather(recv_rows, 'tp', axis=2, tiled=True)  45.2 us
    all_to_all x1, waiting for transfers between devices, body(): lax.all_to_all(slot_grad, 'sp', split_axis=1, concat_axis=0, tiled=True)  17.4 us
    all_to_all x1, blocking collectives, body(): lax.all_to_all(send_rows, 'sp', split_axis=0, concat_axis=1, tiled=True)  16.6 us
    all_gather x1, waiting for transfers between devices, body(): full_mixer_cot = lax.all_gather(mixer_cot, 'tp', axis=1, tiled=True)  16.1 us
    all_to_all x1, blocking collectives, body(): lax.all_to_all(send_cot, 'sp', split_axis=0, concat_axis=1, tiled=True)  13.3 us
    ppermute x2, waiting for transfers between devices, padded(): after = lax.ppermute(initial, axis, down)  11.6 us
  transfers between devices with their start and end apart: 11, of which 6 were waited for; matrix products, arithmetic and copies ran while one was open for 10% of the time, Pallas kernels for 0%

commit v1 on v0

--- a/solution.py
+++ b/solution.py
@@ -1,7 +1,154 @@
 import jax
 import jax.numpy as jnp
 from jax import lax
+from jax.experimental import pallas as pl
+from jax.experimental.pallas import tpu as pltpu
 from jax.sharding import PartitionSpec as P
+
+MESH = pl.DeviceIdType.MESH
+
+
+def peers_of(group):
+    sp, tp = (lax.axis_index("sp"), lax.axis_index("tp"))
+    if group == "core":
+        me, size = (lax.rem(tp, 2), 2)
+    elif group == "z":
+        me, size = (lax.div(tp, 2), lax.axis_size("tp") // 2)
+    else:
+        me, size = (sp, lax.axis_size("sp"))
+    others = []
+    for k in range(1, size):
+        place = lax.rem(me + k, size)
+        if group == "core":
+            others.append((place, (sp, tp - me + place)))
+        elif group == "z":
+            others.append((place, (sp, place * 2 + lax.rem(tp, 2))))
+        else:
+            others.append((place, (place, tp)))
+    return me, others
+
+
+def group_size(group):
+    if group == "core":
+        return 2
+    return lax.axis_size("tp") // 2 if group == "z" else lax.axis_size("sp")
+
+
+def block(ref, place, width):
+    return ref.at[:, pl.ds(pl.multiple_of(place * width, width), width)]
+
+
+def exchange(collective_id, *ops):
+    arrays = [op[2] for op in ops]
+    shapes = []
+    counts = []
+    for kind, group, array, *rest in ops:
+        size = group_size(group)
+        if kind == "cores":
+            shape, count = ((array.shape[0], array.shape[1] // 2), array.shape[1] // rest[0] // 2)
+        elif kind == "columns":
+            shape = (size - 1, array.shape[0], array.shape[1] // size)
+            count = size - 1
+        elif kind == "rows":
+            shape, count = ((size - 1,) + array.shape[1:], size - 1)
+        elif kind == "gather":
+            shape, count = ((array.shape[0], array.shape[1] * size), size - 1)
+        elif kind == "send":
+            shape, count = (array.shape, size - 1)
+        else:
+            shape, count = (array.shape, 1)
+        shapes.append(jax.ShapeDtypeStruct(shape, array.dtype))
+        counts.append(count)
+    total = sum(counts)
+
+    def kernel(*refs):
+        n = len(ops)
+        sources, targets = (refs[:n], refs[n : 2 * n])
+        send_sem, recv_sem, own_sem = refs[2 * n :]
+        barrier = pltpu.get_barrier_semaphore()
+        greeted = 0
+        for group in sorted({op[1] for op in ops}):
+            for _, device in peers_of(group)[1]:
+                pl.semaphore_signal(barrier, inc=1, device_id=device, device_id_type=MESH)
+                greeted += 1
+        pl.semaphore_wait(barrier, greeted)
+        copies = []
+        local = []
+        for i, (kind, group, array, *rest) in enumerate(ops):
+            me, others = peers_of(group)
+            source, target = (sources[i], targets[i])
+            moves = []
+            if kind == "cores":
+                width = rest[0]
+                place, device = others[0]
+                for b in range(counts[i]):
+                    moves.append(
+                        (
+                            block(source, 2 * b + place, width),
+                            target.at[:, pl.ds(b * width, width)],
+                            device,
+                        )
+                    )
+            for k, (place, device) in enumerate(others):
+                if kind == "columns":
+                    moves.append((block(source, place, shapes[i].shape[2]), target.at[k], device))
+                elif kind == "rows":
+                    moves.append((source.at[place], target.at[k], device))
+                elif kind == "gather":
+                    moves.append((source, block(target, me, array.shape[1]), device))
+                elif kind == "send":
+                    moves.append((source.at[place], target.at[me], device))
+                elif kind == "swap":
+                    moves.append((source, target, device))
+            for a, b, device in moves:
+                j = len(copies)
+                copy = pltpu.make_async_remote_copy(
+                    src_ref=a,
+                    dst_ref=b,
+                    send_sem=send_sem.at[j],
+                    recv_sem=recv_sem.at[j],
+                    device_id=device,
+                    device_id_type=MESH,
+                )
+                copy.start()
+                copies.append(copy)
+            if kind == "gather":
+                local.append((source, block(target, me, array.shape[1]), i))
+            elif kind == "send":
+                local.append((source.at[me], target.at[me], i))
+        own = [pltpu.make_async_copy(a, b, own_sem.at[i]) for a, b, i in local]
+        for copy in own:
+            copy.start()
+        for copy in own + copies:
+            copy.wait()
+
+    return pl.pallas_call(
+        kernel,
+        out_shape=shapes,
+        in_specs=[pl.BlockSpec(memory_space=pl.ANY)] * len(ops),
+        out_specs=[pl.BlockSpec(memory_space=pl.ANY)] * len(ops),
+        scratch_shapes=[
+            pltpu.SemaphoreType.DMA((total,)),
+            pltpu.SemaphoreType.DMA((total,)),
+            pltpu.SemaphoreType.DMA((len(ops),)),
+        ],
+        compiler_params=pltpu.CompilerParams(collective_id=collective_id, has_side_effects=True),
+    )(*arrays)
+
+
+def halves(array, width):
+    rows, columns = array.shape
+    split = array.reshape(rows, columns // width // 2, 2, width)
+    core = lax.rem(lax.axis_index("tp"), 2)
+    return jnp.where(core == 0, split[:, :, 0], split[:, :, 1]).reshape(rows, columns // 2)
+
+
+def interleave(own, other, width):
+    rows, columns = own.shape
+    core = lax.rem(lax.axis_index("tp"), 2)
+    own, other = (a.reshape(rows, columns // width, width) for a in (own, other))
+    first, second = (jnp.where(core == 0, own, other), jnp.where(core == 0, other, own))
+    return jnp.stack([first, second], axis=2).reshape(rows, 2 * columns)
 
 
 def padded(array, sides, width):
@@ -96,12 +243,36 @@
     partial_grad = jnp.einsum(
         "prf,pdf->prd", grad_pre_gate, expert_gate, preferred_element_type=jnp.float32
     ) + jnp.einsum("prf,pdf->prd", grad_pre_up, expert_up, preferred_element_type=jnp.float32)
-    slot_grad = lax.psum_scatter(partial_grad, "tp", scatter_dimension=2, tiled=True)
-    returned = lax.all_to_all(slot_grad, "sp", split_axis=1, concat_axis=0, tiled=True)
-    flat_returned = returned.reshape(expert_count * capacity, part_width)
-    moe_grad = jnp.sum(
-        flat_returned[slot_index].reshape(token_count, pick_count, part_width), axis=1
-    )
+    me = lax.axis_index("sp")
+    block_rows = local_count * capacity
+    partial_rows = partial_grad.astype(jnp.bfloat16).reshape(local_count * group_count * capacity, -1)
+    (other_core,) = exchange(1, ("cores", "core", partial_rows, part_width))
+    chip_rows = (
+        halves(partial_rows, part_width).astype(jnp.float32) + other_core.astype(jnp.float32)
+    ).astype(jnp.bfloat16)
+    half = chip_rows.shape[1]
+    chip_rows = jnp.swapaxes(
+        chip_rows.reshape(local_count, group_count, capacity, half), 0, 1
+    ).reshape(group_count, block_rows, half)
+    (returned,) = exchange(2, ("rows", "sp", chip_rows))
+    back = lax.rem(me - jnp.arange(group_count) + group_count, group_count)
+    local_slots = jnp.arange(block_rows, dtype=jnp.int32)
+    picks = jnp.sum(
+        (slot_index.reshape(token_count, pick_count)[None, :, :, None])
+        == (back[:, None] * block_rows + local_slots)[:, None, None, :],
+        axis=2,
+    ).astype(jnp.bfloat16)
+    token_part = jnp.dot(
+        picks[0],
+        lax.dynamic_index_in_dim(chip_rows, me, 0, keepdims=False),
+        preferred_element_type=jnp.float32,
+    ) + jnp.einsum("kts,ksd->td", picks[1:], returned, preferred_element_type=jnp.float32)
+    token_part = token_part.astype(jnp.bfloat16)
+    (parts,) = exchange(3, ("columns", "z", token_part))
+    own_part = lax.dynamic_slice_in_dim(
+        token_part, lax.div(lax.axis_index("tp"), 2) * part_width, part_width, axis=1
+    )
+    moe_grad = own_part.astype(jnp.float32) + jnp.sum(parts.astype(jnp.float32), axis=0)
     mixer_cot = (cotangent.astype(jnp.float32) + moe_grad).astype(jnp.bfloat16)
     conv_in = in_gate.astype(jnp.float32) * values.astype(jnp.float32)
     rimmed = padded(conv_in, (("sp", 0),), 1)

time: 425 us -> 389 us (0.915)
  waiting for transfers between devices: 275 us -> 136 us
  Pallas kernels: 0 us -> 65.7 us
  other arithmetic: 5.71 us -> 36.4 us
  matrix products: 52 us -> 57.7 us
  local copies, waits for them, and re-layouts: 27.5 us -> 33.1 us
    reduce_scatter x1 -> x0, waiting for transfers between devices: 128 us -> none  [body(): lax.psum_scatter(partial_grad, 'tp', scatter_dimension=2, tiled=True)]
    pallas_call x0 -> x3, Pallas kernels: none -> 65.7 us  [exchange(): pl.pallas_call(kernel, out_shape=shapes, in_specs=[pl.BlockSpec(memory_sp...]
    convert_element_type x0 -> x3, other arithmetic: none -> 30.1 us  [the longest x1 27.3 us: body(): halves(partial_rows, part_width).astype(jnp.float32)]
    all_to_all x1 -> x0, waiting for transfers between devices: 17.4 us -> none  [body(): lax.all_to_all(slot_grad, 'sp', split_axis=1, concat_axis=0, tiled=True)]
    another operation x0 -> x1, local copies, waits for them, and re-layouts: none -> 11.4 us  [halves(): split = array.reshape(rows, columns // width // 2, 2, width)]
    dot_general x0 -> x2, matrix products: none -> 5.24 us  [the longest x1 2.67 us: body(): jnp.einsum('kts,ksd->td', picks[1:], returned, preferred_element_type=jnp...]
    all_gather x1, waiting for transfers between devices: 16.1 us -> 21 us  [body(): full_mixer_cot = lax.all_gather(mixer_cot, 'tp', axis=1, tiled=True)]
    unnamed x41 -> x43, local copies, waits for them, and re-layouts: 3.06 us -> 7.72 us
  transfers between devices with their start and end apart: 11 -> 9, of which waited for: 6 -> 5; matrix products, arithmetic and copies ran while one was open for 10% -> 10% of each run, Pallas kernels for 0% -> 0%
where the time goes in v1:
time: 389 us; the launch traced here: 388 us
  waiting for transfers between devices  136 us (35%)
  Pallas kernels  65.7 us (17%)
  matrix products  57.7 us (15%)
  other arithmetic  36.4 us (9%)
  local copies, waits for them, and re-layouts  33.1 us (9%)
  blocking collectives  29.7 us (8%)
  starting transfers between devices  15.1 us (4%)
  between operations  14.2 us (4%)
    pallas_call x3, Pallas kernels, exchange(): pl.pallas_call(kernel, out_shape=shapes, in_specs=[pl.BlockSpec(memory_sp...  65.7 us
    all_gather x1, waiting for transfers between devices, body(): lax.all_gather(recv_cot, 'tp', axis=2, tiled=True)  56.7 us
    all_gather x1, waiting for transfers between devices, body(): lax.all_gather(recv_rows, 'tp', axis=2, tiled=True)  44.6 us
    convert_element_type x1, other arithmetic, body(): halves(partial_rows, part_width).astype(jnp.float32)  27.3 us
    all_gather x1, waiting for transfers between devices, body(): full_mixer_cot = lax.all_gather(mixer_cot, 'tp', axis=1, tiled=True)  21 us
    all_to_all x1, blocking collectives, body(): lax.all_to_all(send_rows, 'sp', split_axis=0, concat_axis=1, tiled=True)  16.4 us
    all_to_all x1, blocking collectives, body(): lax.all_to_all(send_cot, 'sp', split_axis=0, concat_axis=1, tiled=True)  13.2 us
    ppermute x2, waiting for transfers between devices, padded(): after = lax.ppermute(initial, axis, down)  11.8 us
  transfers between devices with their start and end apart: 9, of which 5 were waited for; matrix products, arithmetic and copies ran while one was open for 10% of the time, Pallas kernels for 0%

profile of v1, /device:TPU:0, one launch (start us, length us, event | category | flops | bytes accessed | tf_op | source)
XLA Modules:
  0.0 388.1 jit_solution(15132288588126972892)
XLA Ops:
  17.3 16.4 %all_to_all.43 = bf16[4,192,512]{2,1,0:T(8,128)(2,1)} all-to-all(bf16[4,192,512]{2,1,0:T(8,128)(2,1)S(1)} %bitcast.107), channel_id=1, replica_groups=mesh['sp'=4,'tp'=8] {'sp'}, dimensions={0} | all-to-all | bytes 1572864 | tf_op jit(solution)/shard_map/all_to_all | solution.py:213
  39.7 13.2 %all_to_all.44 = bf16[4,192,512]{2,1,0:T(8,128)(2,1)} all-to-all(bf16[4,192,512]{2,1,0:T(8,128)(2,1)S(1)} %fusion.30), channel_id=1, replica_groups=mesh['sp'=4,'tp'=8] {'sp'}, dimensions={0} | all-to-all | bytes 1572864 | tf_op jit(solution)/shard_map/all_to_all | solution.py:214
  53.7 44.6 %all-gather.7.cloned.1.call-done = bf16[1,768,4096]{2,1,0:T(8,128)(2,1)} async-done(((bf16[1,768,512]{2,1,0:T(8,128)(2,1)}), bf16[1,768,4096]{2,1,0:T(8,128)(2,1)}) %all-gather.7.cloned.1.call-update) | async-done | bytes 6291472 | tf_op jit(solution)/shard_map/all_gather | solution.py:217
  98.3 5.6 %fusion.6 = f32[768,256]{1,0:T(8,128)} fusion(bf16[1,768,4096]{2,1,0:T(8,128)(2,1)} %all-gather.7.cloned.1.call-done, bf16[1,4096,256]{2,1,0:T(8,128)(2,1)S(1)} %copy-done), kind=kOutput, calls=%fused_computation.12 | convolution fusion | flops 1610612736 | bytes 9175040 | tf_op jit(solution)/shard_map/prd,pdf->prf/dot_general | solution.py:220
  106.6 56.7 %all-gather.5.cloned.1.call-done = bf16[1,768,4096]{2,1,0:T(8,128)(2,1)} async-done(((bf16[1,768,512]{2,1,0:T(8,128)(2,1)}), bf16[1,768,4096]{2,1,0:T(8,128)(2,1)}) %all-gather.5.cloned.1.call-update) | async-done | bytes 6291472 | tf_op jit(solution)/shard_map/all_gather | solution.py:218
  163.3 6.5 %multiply_convert_fusion.1 = (bf16[768,256]{1,0:T(8,128)(2,1)}, bf16[768,256]{1,0:T(8,128)(2,1)S(1)}) fusion(f32[768,256]{1,0:T(8,128)} %fusion.6, f32[768,256]{1,0:T(8,128)} %fusion.8, bf16[1,256,4096]{2,1,0:T(8,128)(2,1)} %param.22, bf16[1,768,4096]{2,1,0:T(8,128)(2,1)} %all-gather.5.cloned.1.call-done), kind=kOutput, calls=%fused_computation.41 | convolution fusion | flops 1613168640 | bytes 10747904 | tf_op jit(solution)/shard_map/prd,pfd->prf/dot_general | solution.py:230
  171.7 5.5 %add_convert_fusion.refs_0_ = bf16[768,4096]{1,0:T(8,128)(2,1)} fusion(f32[768,4096]{1,0:T(8,128)S(1)} %fusion.24, bf16[768,256]{1,0:T(8,128)(2,1)} %get-tuple-element.7, bf16[1,4096,256]{2,1,0:T(8,128)(2,1)S(1)} %copy-done.5), kind=kOutput, calls=%fused_computation.4 | convolution fusion | flops 1616904192 | bytes 21364736 | tf_op jit(solution)/shard_map/prf,pdf->prd/dot_general | solution.py:245
  177.2 6.1 %shard_map.171 = bf16[768,2048]{1,0:T(8,128)(2,1)} custom-call(bf16[768,4096]{1,0:T(8,128)(2,1)} %add_convert_fusion.refs_0_), custom_call_target="tpu_custom_call" | custom-call | tf_op jit(solution)/shard_map/pallas_call | solution.py:125
  183.3 11.4 %reshape_reshape.3 = bf16[768,4,2,512]{3,2,1,0:T(2,128)(2,1)} reshape(bf16[768,4096]{1,0:T(8,128)(2,1)} %add_convert_fusion.refs_0_) | data formatting | bytes 12582912 | tf_op jit(solution)/shard_map/reshape;reshape | solution.py:141
  194.6 27.3 %fusion.1 = f32[768,4,512]{2,1,0:T(4,128)} fusion(pred[]{:T(512)S(6)} %eq.52, bf16[768,4,2,512]{3,2,1,0:T(2,128)(2,1)} %reshape_reshape.3), kind=kLoop, calls=%fused_computation.7 | loop fusion | flops 3145728 | bytes 12582913 | tf_op jit(solution)/shard_map/convert_element_type | solution.py:251
  222.0 6.0 %copy.33 = f32[96,8,4,512]{3,1,2,0:T(8,128)S(1)} copy(f32[96,8,4,512]{3,2,1,0:T(4,128)} %bitcast.103) | data formatting | bytes 12582912
  227.9 2.8 add_convert_fusion.1
  230.7 37.9 %shard_map.172 = bf16[3,192,2048]{2,1,0:T(8,128)(2,1)} custom-call(bf16[4,192,2048]{2,1,0:T(8,128)(2,1)} %bitcast.104), custom_call_target="tpu_custom_call" | custom-call | tf_op jit(solution)/shard_map/pallas_call | solution.py:125
  273.8 21.8 %shard_map.173 = bf16[3,256,512]{2,1,0:T(8,128)(2,1)} custom-call(bf16[256,2048]{1,0:T(8,128)(2,1)} %fusion.23.refs_0_), custom_call_target="tpu_custom_call" | custom-call | tf_op jit(solution)/shard_map/pallas_call | solution.py:125
  298.9 2.8 collective-permute-start
  303.3 6.7 %fusion.14 = f32[1,256,4096]{2,1,0:T(8,128)} fusion(bf16[1,768,4096]{2,1,0:T(8,128)(2,1)} %all-gather.5.cloned.1.call-done, f32[768,256]{1,0:T(8,128)S(1)} %copy-done.7, f32[768,256]{1,0:T(8,128)S(1)} %copy-done.6), kind=kOutput, calls=%fused_computation.21 | convolution fusion | flops 1611792384 | bytes 12058624 | tf_op jit(solution)/shard_map/prf,prd->pfd/dot_general | solution.py:227
  310.0 21.0 %all-gather.9.cloned.1.call-done = bf16[256,4096]{1,0:T(8,128)(2,1)} async-done(((bf16[256,512]{1,0:T(8,128)(2,1)}), bf16[256,4096]{1,0:T(8,128)(2,1)}) %all-gather.9.cloned.1.call-update) | async-done | bytes 2097168 | tf_op jit(solution)/shard_map/all_gather | solution.py:281
  331.0 5.5 %fusion.36 = (bf16[256,512]{1,0:T(8,128)(2,1)}, bf16[256,512]{1,0:T(8,128)(2,1)}, f32[256,512]{1,0:T(8,128)S(1)}) fusion(bf16[256,512]{1,0:T(8,128)(2,1)S(1)} %copy-done.19, f32[512]{0:T(512)S(1)} %bitcast.114, f32[1,512]{1,0:T(1,128)S(1)} %collective-permute-done.1, f32[256,512]{1,0:T(8,128)} %copy-done.11, f32[512]{0:T(512)S(1)} %bitcast.116, ...), kind=kOutput, calls=%fused_computation.52 | convolution fusion | flops 1075445760 | bytes 8136704 | tf_op jit(solution)/shard_map/dot_general | solution.py:282
  338.1 4.6 %all-to-all-start.2 = ((bf16[256,4,1024]{2,0,1:T(8,128)(2,1)}), bf16[256,4,1024]{2,0,1:T(8,128)(2,1)}, u32[]{:S(2)}, u32[]{:S(2)}) async-start(bf16[256,4,1024]{2,0,1:T(8,128)(2,1)} %bitcast.98), calls=%async_computation.2 | async-start | bytes 4194304 | tf_op jit(solution)/shard_map/all_to_all | solution.py:291
  342.7 6.8 %fusion.20 = f32[1,4096,256]{2,1,0:T(8,128)} fusion(bf16[768,256]{1,0:T(8,128)(2,1)S(1)} %copy-done.14, bf16[1,768,4096]{2,1,0:T(8,128)(2,1)} %all-gather.7.cloned.1.call-done), kind=kOutput, calls=%fused_computation.23 | convolution fusion | flops 1610612736 | bytes 10878976 | tf_op jit(solution)/shard_map/prd,prf->pdf/dot_general | solution.py:240
  350.8 4.5 %collective-permute-start.3 = (f32[1,512]{1,0:T(1,128)S(1)}, f32[1,512]{1,0:T(1,128)S(1)}, u32[]{:S(2)}, u32[]{:S(2)}) collective-permute-start(f32[1,512]{1,0:T(1,128)S(1)} %get-tuple-element.15), channel_id=1, source_target_pairs={{0,8},{8,16},{16,24},{1,9},{9,17},{17,25},{2,10},{10,18},{18,26},{... | collective-permute-start | bytes 6152 | tf_op jit(solution)/shard_map/ppermute | solution.py:161
  355.4 6.6 %fusion.17 = f32[1,4096,256]{2,1,0:T(8,128)} fusion(bf16[768,256]{1,0:T(8,128)(2,1)S(1)} %copy-done.13, bf16[1,768,4096]{2,1,0:T(8,128)(2,1)} %all-gather.7.cloned.1.call-done), kind=kOutput, calls=%fused_computation.22 | convolution fusion | flops 1610612736 | bytes 10878976 | tf_op jit(solution)/shard_map/prd,prf->pdf/dot_general | solution.py:237
  362.0 11.8 %collective-permute-done.2 = f32[1,512]{1,0:T(1,128)S(1)} collective-permute-done((f32[1,512]{1,0:T(1,128)S(1)}, f32[1,512]{1,0:T(1,128)S(1)}, u32[]{:S(2)}, u32[]{:S(2)}) %collective-permute-start.2) | collective-permute-done | bytes 2080 | tf_op jit(solution)/shard_map/ppermute | solution.py:162
  376.9 4.6 %fusion.65 = f32[1024,512]{1,0:T(8,128)} fusion(bf16[1024,1024]{1,0:T(8,128)(2,1)} %bitcast.20, bf16[1024,512]{1,0:T(8,128)(2,1)} %all-gather.11.cloned.1.call-done), kind=kOutput, calls=%fused_computation.103 | convolution fusion | flops 1073741824 | bytes 5242880 | tf_op jit(solution)/shard_map/dot_general | solution.py:292
  (98 shorter events, 37.2 us)
Async XLA Ops:
  7.2 91.2 %copy-start = (bf16[1,4096,256]{2,1,0:T(8,128)(2,1)S(1)}, bf16[1,4096,256]{2,1,0:T(8,128)(2,1)}, u32[]{:S(2)}) copy-start(bf16[1,4096,256]{2,1,0:T(8,128)(2,1)} %param.20) | copy-start | bytes 6291460
  7.2 91.1 %all-gather.7.cloned.1.call-start = ((), (), s32[]{:S(2)}) async-start(), calls=%async_computation.4 | async-start | bytes 7077888 | tf_op jit(solution)/shard_map/all_gather | solution.py:217
  14.6 19.2 %copy-start.16 = (f32[256,2]{0,1:T(2,128)S(1)}, f32[256,2]{0,1:T(2,128)}, u32[]{:S(2)}) copy-start(f32[256,2]{0,1:T(2,128)} %param.19) | copy-start | bytes 6148
  14.6 22.2 %copy-start.8 = (bf16[256,512]{1,0:T(8,128)(2,1)S(1)}, bf16[256,512]{1,0:T(8,128)(2,1)}, u32[]{:S(2)}) copy-start(bf16[256,512]{1,0:T(8,128)(2,1)} %param.23) | copy-start | bytes 786436
  33.8 129.5 %all-gather.5.cloned.1.call-start = ((), (), s32[]{:S(2)}) async-start(), calls=%async_computation.3 | async-start | bytes 7077888 | tf_op jit(solution)/shard_map/all_gather | solution.py:218
  53.0 278.0 %all-gather.9.cloned.1.call-start = ((), (), s32[]{:S(2)}) async-start(), calls=%async_computation.5 | async-start | bytes 2359296 | tf_op jit(solution)/shard_map/all_gather | solution.py:281
  98.3 5.6 %copy-start.4 = (bf16[1,4096,256]{2,1,0:T(8,128)(2,1)S(1)}, bf16[1,4096,256]{2,1,0:T(8,128)(2,1)}, u32[]{:S(2)}) copy-start(bf16[1,4096,256]{2,1,0:T(8,128)(2,1)} %param.21) | copy-start | bytes 6291460
  98.3 5.6 %copy-start.18 = (bf16[1,768,4096]{2,1,0:T(8,128)(2,1)S(1)}, bf16[1,768,4096]{2,1,0:T(8,128)(2,1)}, u32[]{:S(2)}) copy-start(bf16[1,768,4096]{2,1,0:T(8,128)(2,1)} %all-gather.7.cloned.1.call-done) | copy-start | bytes 18874372
  221.9 6.0 %copy-start.2 = (bf16[768,2048]{1,0:T(8,128)(2,1)S(1)}, bf16[768,2048]{1,0:T(8,128)(2,1)}, u32[]{:S(2)}) copy-start(bf16[768,2048]{1,0:T(8,128)(2,1)} %shard_map.171) | copy-start | bytes 9437188
  273.8 25.0 %copy-start.9 = (bf16[256,512]{1,0:T(8,128)(2,1)S(1)}, bf16[256,512]{1,0:T(8,128)(2,1)}, u32[]{:S(2)}) copy-start(bf16[256,512]{1,0:T(8,128)(2,1)} %param.15) | copy-start | bytes 786436
  273.8 25.0 %copy-start.10 = (bf16[256,512]{1,0:T(8,128)(2,1)S(1)}, bf16[256,512]{1,0:T(8,128)(2,1)}, u32[]{:S(2)}) copy-start(bf16[256,512]{1,0:T(8,128)(2,1)} %param.14) | copy-start | bytes 786436
  273.8 29.4 %copy-start.15 = (f32[3,512]{1,0:T(4,128)S(1)}, f32[3,512]{1,0:T(4,128)}, u32[]{:S(2)}) copy-start(f32[3,512]{1,0:T(4,128)} %param.16) | copy-start | bytes 18436
  273.8 29.4 %copy-start.6 = (f32[768,256]{1,0:T(8,128)S(1)}, f32[768,256]{1,0:T(8,128)}, u32[]{:S(2)}) copy-start(f32[768,256]{1,0:T(8,128)} %fusion.6) | copy-start | bytes 2359300
  273.8 29.4 %copy-start.7 = (f32[768,256]{1,0:T(8,128)S(1)}, f32[768,256]{1,0:T(8,128)}, u32[]{:S(2)}) copy-start(f32[768,256]{1,0:T(8,128)} %fusion.8) | copy-start | bytes 2359300
  298.7 78.2 %all-gather.11.cloned.1.call-start = ((), (), s32[]{:S(2)}) async-start(), calls=%async_computation.6 | async-start | bytes 1310720 | tf_op jit(solution)/shard_map/all_gather | solution.py:294
  298.9 11.1 %copy-start.11 = (f32[256,512]{1,0:T(8,128)}, f32[256,512]{1,0:T(8,128)S(1)}, u32[]{:S(2)}) copy-start(f32[256,512]{1,0:T(8,128)S(1)} %convert_multiply_fusion.4) | copy-start | bytes 1572868
  298.9 11.1 %collective-permute-start = (f32[1,512]{1,0:T(1,128)S(1)}, f32[1,512]{1,0:T(1,128)S(1)}, u32[]{:S(2)}, u32[]{:S(2)}) collective-permute-start(f32[1,512]{1,0:T(1,128)S(1)} %get-tuple-element.16), channel_id=1, source_target_pairs={{0,8},{8,16},{16,24},{1,9},{9,17},{17,25},{2,10},{10,18},{18,26},{... | collective-permute-start | bytes 6152 | tf_op jit(solution)/shard_map/ppermute | solution.py:161
  301.7 8.4 %collective-permute-start.1 = (f32[1,512]{1,0:T(1,128)S(1)}, f32[1,512]{1,0:T(1,128)S(1)}, u32[]{:S(2)}, u32[]{:S(2)}) collective-permute-start(f32[1,512]{1,0:T(1,128)S(1)} %get-tuple-element.17), channel_id=1, source_target_pairs={{8,0},{16,8},{24,16},{9,1},{17,9},{25,17},{10,2},{18,10},{26,18},{... | collective-permute-start | bytes 6152 | tf_op jit(solution)/shard_map/ppermute | solution.py:162
  303.3 27.7 %copy-start.19 = (bf16[256,512]{1,0:T(8,128)(2,1)S(1)}, bf16[256,512]{1,0:T(8,128)(2,1)}, u32[]{:S(2)}) copy-start(bf16[256,512]{1,0:T(8,128)(2,1)} %param.13) | copy-start | bytes 786436
  331.0 5.5 %copy-start.3 = (bf16[256,4096]{1,0:T(8,128)(2,1)S(1)}, bf16[256,4096]{1,0:T(8,128)(2,1)}, u32[]{:S(2)}) copy-start(bf16[256,4096]{1,0:T(8,128)(2,1)} %all-gather.9.cloned.1.call-done) | copy-start | bytes 6291460
  338.1 38.8 %all-to-all-start.2 = ((bf16[256,4,1024]{2,0,1:T(8,128)(2,1)}), bf16[256,4,1024]{2,0,1:T(8,128)(2,1)}, u32[]{:S(2)}, u32[]{:S(2)}) async-start(bf16[256,4,1024]{2,0,1:T(8,128)(2,1)} %bitcast.98), calls=%async_computation.2 | async-start | bytes 4194304 | tf_op jit(solution)/shard_map/all_to_all | solution.py:291
  342.7 12.7 %copy-start.13 = (bf16[768,256]{1,0:T(8,128)(2,1)S(1)}, bf16[768,256]{1,0:T(8,128)(2,1)}, u32[]{:S(2)}) copy-start(bf16[768,256]{1,0:T(8,128)(2,1)} %copy-done.12) | copy-start | bytes 1179652
  349.5 24.3 %collective-permute-start.2 = (f32[1,512]{1,0:T(1,128)S(1)}, f32[1,512]{1,0:T(1,128)S(1)}, u32[]{:S(2)}, u32[]{:S(2)}) collective-permute-start(f32[1,512]{1,0:T(1,128)S(1)} %get-tuple-element.14), channel_id=1, source_target_pairs={{8,0},{16,8},{24,16},{9,1},{17,9},{25,17},{10,2},{18,10},{26,18},{... | collective-permute-start | bytes 6152 | tf_op jit(solution)/shard_map/ppermute | solution.py:162
  350.8 23.0 %collective-permute-start.3 = (f32[1,512]{1,0:T(1,128)S(1)}, f32[1,512]{1,0:T(1,128)S(1)}, u32[]{:S(2)}, u32[]{:S(2)}) collective-permute-start(f32[1,512]{1,0:T(1,128)S(1)} %get-tuple-element.15), channel_id=1, source_target_pairs={{0,8},{8,16},{16,24},{1,9},{9,17},{17,25},{2,10},{10,18},{18,26},{... | collective-permute-start | bytes 6152 | tf_op jit(solution)/shard_map/ppermute | solution.py:161
  (5 other events, 13.5 us)
Sparse Core Ops, SparseCore 0:
  33.9 64.3 all-gather.6
  99.9 63.3 all-gather.4
  298.8 32.1 all-gather.8
  336.7 40.2 all-gather.10
